TPU v7x, 32 devices: a whole 2x2x4 slice. The times are simulated.
32 devices in a mesh: fs: 8 (over z, x), tp: 4 (over y, core).
Axes of the slice: x: 2, y: 2, z: 4, core: 2. Of those that a mesh axis runs over, the one named last changes fastest.
Arguments:
- normed_input: bfloat16 [16384, 2048], P('fs'), may hold values from -6 to 6
- output_cotangent: bfloat16 [16384, 2048], P('fs'), may hold values from -6 to 6
- query_grad: bfloat16 [16384, 2048], P('fs', 'tp'), may hold values from -0.75 to 0.75
- key_grad: bfloat16 [16384, 2048], P('fs', 'tp'), may hold values from -0.75 to 0.75
- attn_values: bfloat16 [16384, 2048], P('fs', 'tp'), may hold values from -0.75 to 0.75
- master_weights: float32 [3, 2048, 2048], P(None, 'fs', 'tp'), may hold values from -3 to 3
- factors: bfloat16 [3, 2048, 256], P(None, 'fs'), may hold values from -0.375 to 0.375
- moments: float32 [3, 256, 2048], P(None, 'fs', 'tp'), may hold values from -620 to 620
Outputs:
- new_weights: float32 [3, 2048, 2048], P(None, 'fs', 'tp')
- weight_copies: bfloat16 [3, 2048, 2048], P(None, None, 'tp')
- steps: float32 [3, 2048, 2048], P(None, 'fs', 'tp')
- new_moments: float32 [3, 256, 2048], P(None, 'fs', 'tp')
All inputs are finite; a program needn't handle non-finite values.
Results may differ from a plain program's by a relative error of at most 0.0055.
Values may be sent and summed in bfloat16 or wider, within the bound.
A program may use at most 128 MiB of HBM per device.

v0:
```python
import jax
import jax.numpy as jnp
from jax import lax
from jax.sharding import PartitionSpec as P


def on_device(
    normed_input,
    output_cotangent,
    query_grad,
    key_grad,
    attn_values,
    master_weights,
    factors,
    moments,
):
    rank_rows = moments.shape[1]
    width = query_grad.shape[1]
    rank = factors.shape[2]
    contract = (((0,), (0,)), ((), ()))
    whole_factors = lax.all_gather(factors, "fs", axis=1, tiled=True)
    reduced = [
        jnp.dot(normed_input, whole_factors[0], preferred_element_type=jnp.float32),
        jnp.dot(normed_input, whole_factors[1], preferred_element_type=jnp.float32),
        jnp.dot(output_cotangent, whole_factors[2], preferred_element_type=jnp.float32),
    ]
    head_sides = [query_grad, key_grad, attn_values]
    pieces = []
    for index in range(3):
        reduced_cols = reduced[index]
        pieces.append(
            lax.dot_general(
                reduced_cols,
                head_sides[index].astype(jnp.float32),
                contract,
                precision=lax.Precision.HIGHEST,
                preferred_element_type=jnp.float32,
            )
        )
    projected = lax.psum_scatter(
        jnp.concatenate(pieces, axis=1).astype(jnp.bfloat16), "fs", scatter_dimension=0, tiled=True
    ).astype(jnp.float32)
    split = projected.reshape(rank_rows, 3, width).transpose(1, 0, 2)
    new_moments = 0.8 * moments + 0.2 * split
    total = lax.psum(jnp.sum(new_moments * new_moments), ("fs", "tp"))
    entries = 3 * rank * width * lax.axis_size("tp")
    rms = jnp.sqrt(total / entries + 1e-06)
    normalized = (new_moments / rms).astype(jnp.bfloat16)
    gathered = lax.all_gather(normalized, "fs", axis=1, tiled=True)
    steps = jnp.einsum("jdr,jrc->jdc", factors, gathered, preferred_element_type=jnp.float32)
    new_weights = master_weights - 0.05 * steps
    weight_copies = lax.all_gather(new_weights.astype(jnp.bfloat16), "fs", axis=1, tiled=True)
    return (new_weights, weight_copies, steps, new_moments)


def solution(mesh):
    in_specs = (
        P("fs", None),
        P("fs", None),
        P("fs", "tp"),
        P("fs", "tp"),
        P("fs", "tp"),
        P(None, "fs", "tp"),
        P(None, "fs", None),
        P(None, "fs", "tp"),
    )
    out_specs = (P(None, "fs", "tp"), P(None, None, "tp"), P(None, "fs", "tp"), P(None, "fs", "tp"))
    return jax.shard_map(
        on_device, mesh=mesh, in_specs=in_specs, out_specs=out_specs, check_vma=False
    )
```

profile of v0, /device:TPU:0, one launch (start us, length us, event | category | flops | bytes accessed | tf_op | source)
XLA Modules:
  0.0 345.6 jit_solution(5577929369961026899)
XLA Ops:
  7.2 0.0 copy-start
  7.2 0.0 all-gather.3.cloned.1.call-start
  7.2 0.7 all-gather.3.cloned.1.call-update
  7.9 0.0 reduce-scatter.2.cloned.1.call-start
  8.0 65.0 %all-gather.3.cloned.1.call-done = bf16[3,2048,256]{2,1,0:T(8,128)(2,1)} async-done(((bf16[3,256,256]{2,1,0:T(8,128)(2,1)}), bf16[3,2048,256]{2,1,0:T(8,128)(2,1)}) %all-gather.3.cloned.1.call-update) | async-done | bytes 3145744 | tf_op jit(solution)/shard_map/all_gather | solution.py:21
  72.9 6.2 %fusion = f32[2048,256]{1,0:T(8,128)S(1)} fusion(bf16[2048,2048]{1,0:T(8,128)(2,1)} %param.9, bf16[3,2048,256]{2,1,0:T(8,128)(2,1)} %all-gather.3.cloned.1.call-done), kind=kOutput, calls=%fused_computation.6 | convolution fusion | flops 2147483648 | bytes 11534336 | tf_op jit(solution)/shard_map/dot_general | solution.py:25
  79.2 0.0 copy-done
  79.2 1.9 convolution_convert_fusion
  81.2 0.0 copy-start.1
  81.2 2.5 fusion.1
  83.7 1.8 convolution_convert_fusion.1
  85.5 0.0 copy-start.2
  85.5 2.5 fusion.2
  88.0 0.0 copy-done.2
  88.0 2.0 convolution_convert_fusion.2
  90.0 0.9 pad_maximum_fusion
  91.0 0.0 reduce-scatter.2.cloned.1.call-update
  91.0 0.0 copy-start.3
  91.0 0.0 all-gather.5.cloned.1.call-start
  91.1 3.1 copy.18
  94.2 58.9 %reduce-scatter.2.cloned.1.call-done = bf16[32,1536]{1,0:T(8,128)(2,1)} async-done(((bf16[256,1536]{1,0:T(8,128)(2,1)}), bf16[32,1536]{1,0:T(8,128)(2,1)}) %reduce-scatter.2.cloned.1.call-update) | async-done | bytes 98320 | tf_op jit(solution)/shard_map/reduce_scatter | solution.py:40
  153.1 0.9 convert_multiply_fusion
  154.0 0.7 multiply_reduce_fusion
  154.7 40.0 %psum.7 = f32[]{:T(128)} all-reduce(f32[]{:T(128)} %get-tuple-element.14), channel_id=1, replica_groups=mesh['fs'=8,'tp'=4] {'fs','tp'}, use_global_device_ids=true, to_apply=%region_2.0 | all-reduce | flops 1 | bytes 8 | tf_op jit(solution)/shard_map/psum | solution.py:45
  195.4 32.0 %all_gather.10 = bf16[3,256,512]{2,1,0:T(8,128)(2,1)S(1)} all-gather(bf16[3,32,512]{2,1,0:T(8,128)(2,1)S(1)} %divide_convert_fusion), channel_id=1, replica_groups=mesh['fs'=8,'tp'=4] {'fs'}, dimensions={1}, use_global_device_ids=true | all-gather | bytes 884736 | tf_op jit(solution)/shard_map/all_gather | solution.py:49
  227.5 0.0 copy-done.3
  227.5 3.9 %fusion.4 = (bf16[3,256,512]{1,2,0:T(8,128)(2,1)}, f32[3,256,512]{1,2,0:T(8,128)}, f32[3,256,512]{1,2,0:T(8,128)}) fusion(f32[3,256,512]{1,2,0:T(8,128)} %copy.18, bf16[3,256,512]{2,1,0:T(8,128)(2,1)S(1)} %all_gather.10, bf16[3,256,256]{2,1,0:T(8,128)(2,1)S(1)} %copy-done.3), kind=kOutput, calls=%fused_computation.17 | convolution fusion | flops 202506240 | bytes 6684672 | tf_op jit(solution)/shard_map/jdr,jrc->jdc/dot_general | solution.py:50
  231.3 0.0 all-gather.5.cloned.1.call-update
  231.4 3.0 copy.19
  234.4 3.0 copy.21
  237.4 93.1 %all-gather.5.cloned.1.call-done = bf16[3,2048,512]{1,2,0:T(8,128)(2,1)} async-done(((bf16[3,256,512]{1,2,0:T(8,128)(2,1)}), bf16[3,2048,512]{1,2,0:T(8,128)(2,1)}) %all-gather.5.cloned.1.call-update) | async-done | bytes 6291472 | tf_op jit(solution)/shard_map/all_gather | solution.py:52
  330.5 8.6 %copy.20 = bf16[3,2048,512]{2,1,0:T(8,128)(2,1)} copy(bf16[3,2048,512]{1,2,0:T(8,128)(2,1)} %all-gather.5.cloned.1.call-done) | data formatting | bytes 12582912
  (10 shorter events, 0.0 us)
Async XLA Ops:
  7.2 72.0 %copy-start = (bf16[2048,512]{1,0:T(8,128)(2,1)S(1)}, bf16[2048,512]{1,0:T(8,128)(2,1)}, u32[]{:S(2)}) copy-start(bf16[2048,512]{1,0:T(8,128)(2,1)} %param.12) | copy-start | bytes 6291460
  7.2 65.8 %all-gather.3.cloned.1.call-start = ((), (), s32[]{:S(2)}) async-start(), calls=%async_computation.1 | async-start | bytes 3538944 | tf_op jit(solution)/shard_map/all_gather | solution.py:21
  7.9 145.2 %reduce-scatter.2.cloned.1.call-start = ((), (), s32[]{:S(2)}) async-start(), calls=%async_computation.2 | async-start | bytes 884736 | tf_op jit(solution)/shard_map/reduce_scatter | solution.py:40
  72.9 8.2 %copy-start.6 = (bf16[2048,2048]{1,0:T(8,128)(2,1)S(1)}, bf16[2048,2048]{1,0:T(8,128)(2,1)}, u32[]{:S(2)}) copy-start(bf16[2048,2048]{1,0:T(8,128)(2,1)} %param.8) | copy-start | bytes 25165828
  79.2 2.0 copy-start.7
  81.2 2.5 copy-start.1
  85.5 2.5 copy-start.2
  91.0 63.0 %copy-start.5 = (f32[3,32,512]{2,1,0:T(8,128)S(1)}, f32[3,32,512]{2,1,0:T(8,128)}, u32[]{:S(2)}) copy-start(f32[3,32,512]{2,1,0:T(8,128)} %param.15) | copy-start | bytes 589828
  91.0 136.5 %copy-start.3 = (bf16[3,256,256]{2,1,0:T(8,128)(2,1)S(1)}, bf16[3,256,256]{2,1,0:T(8,128)(2,1)}, u32[]{:S(2)}) copy-start(bf16[3,256,256]{2,1,0:T(8,128)(2,1)} %param.14) | copy-start | bytes 1179652
  91.0 239.5 %all-gather.5.cloned.1.call-start = ((), (), s32[]{:S(2)}) async-start(), calls=%async_computation.3 | async-start | bytes 7077888 | tf_op jit(solution)/shard_map/all_gather | solution.py:52
  154.7 76.7 %copy-start.4 = (f32[3,32,512]{2,1,0:T(8,128)}, f32[3,32,512]{2,1,0:T(8,128)S(1)}, u32[]{:S(2)}) copy-start(f32[3,32,512]{2,1,0:T(8,128)S(1)} %get-tuple-element.15) | copy-start | bytes 589828
Sparse Core Ops, SparseCore 0:
  10.2 62.7 all-gather.2
  91.1 61.9 reduce-scatter.1
  231.5 98.9 all-gather.4
where the time goes:
time: 346 us
  waiting for transfers between devices  218 us (63%)
  blocking collectives  72.1 us (21%)
  matrix products  20.8 us (6%)
  local copies, waits for them, and re-layouts  17.8 us (5%)
  between operations  14.6 us (4%)
    all_gather x1, waiting for transfers between devices, on_device(): lax.all_gather(new_weights.astype(jnp.bfloat16), 'fs', axis=1, tiled=True)  93.1 us
    all_gather x1, waiting for transfers between devices, on_device(): whole_factors = lax.all_gather(factors, 'fs', axis=1, tiled=True)  65 us
    reduce_scatter x1, waiting for transfers between devices, on_device(): lax.psum_scatter(jnp.concatenate(pieces, axis=1).astype(jnp.bfloat16), 'f...  58.9 us
    psum x1, blocking collectives, on_device(): total = lax.psum(jnp.sum(new_moments * new_moments), ('fs', 'tp'))  40 us
    all_gather x1, blocking collectives, on_device(): gathered = lax.all_gather(normalized, 'fs', axis=1, tiled=True)  32 us
    unnamed x20, local copies, waits for them, and re-layouts  17.8 us
  transfers between devices with their start and end apart: 3, of which 3 were waited for; matrix products, arithmetic and copies ran while one was open for 3% of the time, Pallas kernels for 0%

commit v1 on v0

--- a/solution.py
+++ b/solution.py
@@ -2,6 +2,18 @@
 import jax.numpy as jnp
 from jax import lax
 from jax.sharding import PartitionSpec as P
+
+
+def product_in_turn(x, axis, dim, term):
+    size, index, width = (lax.axis_size(axis), lax.axis_index(axis), x.shape[dim])
+    right = [(i, (i + 1) % size) for i in range(size)]
+    current, running = (x, None)
+    for step in range(size):
+        following = lax.ppermute(current, axis, right) if step < size - 1 else None
+        take_in = term(current, (index - step) % size * width)
+        running = take_in if running is None else running + take_in
+        current = following
+    return running
 
 
 def on_device(
@@ -46,8 +58,17 @@
     entries = 3 * rank * width * lax.axis_size("tp")
     rms = jnp.sqrt(total / entries + 1e-06)
     normalized = (new_moments / rms).astype(jnp.bfloat16)
-    gathered = lax.all_gather(normalized, "fs", axis=1, tiled=True)
-    steps = jnp.einsum("jdr,jrc->jdc", factors, gathered, preferred_element_type=jnp.float32)
+    steps = product_in_turn(
+        normalized,
+        "fs",
+        1,
+        lambda shard, at: jnp.einsum(
+            "jdr,jrc->jdc",
+            lax.dynamic_slice_in_dim(factors, at, shard.shape[1], axis=2),
+            shard,
+            preferred_element_type=jnp.float32,
+        ),
+    )
     new_weights = master_weights - 0.05 * steps
     weight_copies = lax.all_gather(new_weights.astype(jnp.bfloat16), "fs", axis=1, tiled=True)
     return (new_weights, weight_copies, steps, new_moments)

time: 346 us -> 360 us (1.040)
  waiting for transfers between devices: 218 us -> 272 us
  blocking collectives: 72.1 us -> 40.1 us
  local copies, waits for them, and re-layouts: 17.8 us -> 5.94 us
    ppermute x0 -> x7, waiting for transfers between devices: none -> 46.9 us  [product_in_turn(): following = lax.ppermute(current, axis, right) if step < size - 1 else None]
    all_gather x1 -> x0, blocking collectives: 32 us -> none  [on_device(): gathered = lax.all_gather(normalized, 'fs', axis=1, tiled=True)]
    unnamed x20 -> x19, local copies, waits for them, and re-layouts: 17.8 us -> 5.94 us
    all_gather x1, waiting for transfers between devices: 93.1 us -> 97.2 us  [on_device(): lax.all_gather(new_weights.astype(jnp.bfloat16), 'fs', axis=1, tiled=True)]
  transfers between devices with their start and end apart: 3 -> 10, of which waited for: 3 -> 10; matrix products, arithmetic and copies ran while one was open for 3% -> 1% of each run, Pallas kernels for 0% -> 0%
where the time goes in v1:
time: 360 us
  waiting for transfers between devices  272 us (76%)
  blocking collectives  40.1 us (11%)
  matrix products  22.5 us (6%)
  between operations  14.8 us (4%)
  local copies, waits for them, and re-layouts  5.94 us (2%)
    all_gather x1, waiting for transfers between devices, on_device(): lax.all_gather(new_weights.astype(jnp.bfloat16), 'fs', axis=1, tiled=True)  97.2 us
    all_gather x1, waiting for transfers between devices, on_device(): whole_factors = lax.all_gather(factors, 'fs', axis=1, tiled=True)  65 us
    reduce_scatter x1, waiting for transfers between devices, on_device(): lax.psum_scatter(jnp.concatenate(pieces, axis=1).astype(jnp.bfloat16), 'f...  61.9 us
    ppermute x7, waiting for transfers between devices, product_in_turn(): following = lax.ppermute(current, axis, right) if step < size - 1 else None  46.9 us
    psum x1, blocking collectives, on_device(): total = lax.psum(jnp.sum(new_moments * new_moments), ('fs', 'tp'))  40.1 us
  transfers between devices with their start and end apart: 10, of which 10 were waited for; matrix products, arithmetic and copies ran while one was open for 1% of the time, Pallas kernels for 0%

profile of v1, /device:TPU:0, one launch (start us, length us, event | category | flops | bytes accessed | tf_op | source)
XLA Modules:
  0.0 360.0 jit_solution(11589937479913070164)
XLA Ops:
  7.2 0.7 all-gather.3.cloned.1.call-update
  8.0 65.0 %all-gather.3.cloned.1.call-done = bf16[3,2048,256]{2,1,0:T(8,128)(2,1)} async-done(((bf16[3,256,256]{2,1,0:T(8,128)(2,1)}), bf16[3,2048,256]{2,1,0:T(8,128)(2,1)}) %all-gather.3.cloned.1.call-update) | async-done | bytes 3145744 | tf_op jit(solution)/shard_map/all_gather | solution.py:33
  72.9 6.2 %fusion = f32[2048,256]{1,0:T(8,128)S(1)} fusion(bf16[2048,2048]{1,0:T(8,128)(2,1)} %param.9, bf16[3,2048,256]{2,1,0:T(8,128)(2,1)} %all-gather.3.cloned.1.call-done), kind=kOutput, calls=%fused_computation.6 | convolution fusion | flops 2147483648 | bytes 11534336 | tf_op jit(solution)/shard_map/dot_general | solution.py:37
  79.2 1.9 convolution_convert_fusion
  81.2 2.5 fusion.1
  83.7 1.8 convolution_convert_fusion.1
  85.5 2.5 fusion.2
  88.0 2.0 convolution_convert_fusion.2
  90.1 0.9 pad_maximum_fusion
  91.0 0.0 all-gather.5.cloned.1.call-start
  91.2 61.9 %reduce-scatter.2.cloned.1.call-done = bf16[32,1536]{1,0:T(8,128)(2,1)} async-done(((bf16[256,1536]{1,0:T(8,128)(2,1)}), bf16[32,1536]{1,0:T(8,128)(2,1)}) %reduce-scatter.2.cloned.1.call-update) | async-done | bytes 98320 | tf_op jit(solution)/shard_map/reduce_scatter | solution.py:52
  153.1 0.9 convert_multiply_fusion
  154.0 0.7 multiply_reduce_fusion
  154.7 40.1 %psum.7 = f32[]{:T(128)} all-reduce(f32[]{:T(128)} %get-tuple-element.6), channel_id=1, replica_groups=mesh['fs'=8,'tp'=4] {'fs','tp'}, use_global_device_ids=true, to_apply=%region_2.0 | all-reduce | flops 1 | bytes 8 | tf_op jit(solution)/shard_map/psum | solution.py:57
  195.5 2.3 collective-permute-start
  197.8 0.4 fusion.17
  198.2 4.6 %collective-permute-done = bf16[3,32,512]{2,1,0:T(8,128)(2,1)S(1)} collective-permute-done((bf16[3,32,512]{2,1,0:T(8,128)(2,1)S(1)}, bf16[3,32,512]{2,1,0:T(8,128)(2,1)S(1)}, u32[]{:S(2)}, u32[]{:S(2)}) %collective-permute-start) | collective-permute-done | bytes 98336 | tf_op jit(solution)/shard_map/ppermute | solution.py:12
  202.9 0.4 fusion.15
  203.3 6.9 %collective-permute-done.1 = bf16[3,32,512]{2,1,0:T(8,128)(2,1)S(1)} collective-permute-done((bf16[3,32,512]{2,1,0:T(8,128)(2,1)S(1)}, bf16[3,32,512]{2,1,0:T(8,128)(2,1)S(1)}, u32[]{:S(2)}, u32[]{:S(2)}) %collective-permute-start.1) | collective-permute-done | bytes 98336 | tf_op jit(solution)/shard_map/ppermute | solution.py:12
  210.2 0.4 fusion.13
  210.6 6.9 %collective-permute-done.2 = bf16[3,32,512]{2,1,0:T(8,128)(2,1)S(1)} collective-permute-done((bf16[3,32,512]{2,1,0:T(8,128)(2,1)S(1)}, bf16[3,32,512]{2,1,0:T(8,128)(2,1)S(1)}, u32[]{:S(2)}, u32[]{:S(2)}) %collective-permute-start.2) | collective-permute-done | bytes 98336 | tf_op jit(solution)/shard_map/ppermute | solution.py:12
  217.5 0.4 fusion.11
  217.9 7.0 %collective-permute-done.3 = bf16[3,32,512]{2,1,0:T(8,128)(2,1)S(1)} collective-permute-done((bf16[3,32,512]{2,1,0:T(8,128)(2,1)S(1)}, bf16[3,32,512]{2,1,0:T(8,128)(2,1)S(1)}, u32[]{:S(2)}, u32[]{:S(2)}) %collective-permute-start.3) | collective-permute-done | bytes 98336 | tf_op jit(solution)/shard_map/ppermute | solution.py:12
  224.9 0.4 fusion.9
  225.3 7.7 %collective-permute-done.4 = bf16[3,32,512]{2,1,0:T(8,128)(2,1)S(1)} collective-permute-done((bf16[3,32,512]{2,1,0:T(8,128)(2,1)S(1)}, bf16[3,32,512]{2,1,0:T(8,128)(2,1)S(1)}, u32[]{:S(2)}, u32[]{:S(2)}) %collective-permute-start.4) | collective-permute-done | bytes 98336 | tf_op jit(solution)/shard_map/ppermute | solution.py:12
  233.1 0.4 fusion.7
  233.5 6.9 %collective-permute-done.5 = bf16[3,32,512]{2,1,0:T(8,128)(2,1)S(1)} collective-permute-done((bf16[3,32,512]{2,1,0:T(8,128)(2,1)S(1)}, bf16[3,32,512]{2,1,0:T(8,128)(2,1)S(1)}, u32[]{:S(2)}, u32[]{:S(2)}) %collective-permute-start.5) | collective-permute-done | bytes 98336 | tf_op jit(solution)/shard_map/ppermute | solution.py:12
  240.4 0.4 fusion.5
  240.8 6.9 %collective-permute-done.6 = bf16[3,32,512]{2,1,0:T(8,128)(2,1)S(1)} collective-permute-done((bf16[3,32,512]{2,1,0:T(8,128)(2,1)S(1)}, bf16[3,32,512]{2,1,0:T(8,128)(2,1)S(1)}, u32[]{:S(2)}, u32[]{:S(2)}) %collective-permute-start.6) | collective-permute-done | bytes 98336 | tf_op jit(solution)/shard_map/ppermute | solution.py:12
  247.7 2.7 fusion.27
  250.4 97.2 %all-gather.5.cloned.1.call-done = bf16[3,2048,512]{2,1,0:T(8,128)(2,1)} async-done(((bf16[3,256,512]{2,1,0:T(8,128)(2,1)}), bf16[3,2048,512]{2,1,0:T(8,128)(2,1)}) %all-gather.5.cloned.1.call-update) | async-done | bytes 6291472 | tf_op jit(solution)/shard_map/all_gather | solution.py:73
  347.6 5.9 %copy.42 = bf16[3,2048,512]{2,1,0:T(8,128)(2,1)} copy(bf16[3,2048,512]{2,1,0:T(8,128)(2,1)} %all-gather.5.cloned.1.call-done) | data formatting | bytes 12582912
  (29 shorter events, 0.2 us)
Async XLA Ops:
  7.2 72.0 %copy-start = (bf16[2048,512]{1,0:T(8,128)(2,1)S(1)}, bf16[2048,512]{1,0:T(8,128)(2,1)}, u32[]{:S(2)}) copy-start(bf16[2048,512]{1,0:T(8,128)(2,1)} %param.12) | copy-start | bytes 6291460
  7.2 65.8 %all-gather.3.cloned.1.call-start = ((), (), s32[]{:S(2)}) async-start(), calls=%async_computation.1 | async-start | bytes 3538944 | tf_op jit(solution)/shard_map/all_gather | solution.py:33
  7.9 145.2 %reduce-scatter.2.cloned.1.call-start = ((), (), s32[]{:S(2)}) async-start(), calls=%async_computation.2 | async-start | bytes 884736 | tf_op jit(solution)/shard_map/reduce_scatter | solution.py:52
  72.9 8.2 %copy-start.7 = (bf16[2048,2048]{1,0:T(8,128)(2,1)S(1)}, bf16[2048,2048]{1,0:T(8,128)(2,1)}, u32[]{:S(2)}) copy-start(bf16[2048,2048]{1,0:T(8,128)(2,1)} %param.8) | copy-start | bytes 25165828
  79.2 2.0 copy-start.8
  81.2 2.5 copy-start.2
  85.5 2.5 copy-start.3
  90.0 64.0 %copy-start.6 = (f32[3,32,512]{2,1,0:T(8,128)S(1)}, f32[3,32,512]{2,1,0:T(8,128)}, u32[]{:S(2)}) copy-start(f32[3,32,512]{2,1,0:T(8,128)} %param.15) | copy-start | bytes 589828
  90.1 107.8 %copy-start.1 = (bf16[3,256,256]{2,1,0:T(8,128)(2,1)S(1)}, bf16[3,256,256]{2,1,0:T(8,128)(2,1)}, u32[]{:S(2)}) copy-start(bf16[3,256,256]{2,1,0:T(8,128)(2,1)} %param.14) | copy-start | bytes 1179652
  91.0 256.6 %all-gather.5.cloned.1.call-start = ((), (), s32[]{:S(2)}) async-start(), calls=%async_computation.3 | async-start | bytes 7077888 | tf_op jit(solution)/shard_map/all_gather | solution.py:73
  154.7 55.9 %copy-start.5 = (f32[3,32,512]{2,1,0:T(8,128)}, f32[3,32,512]{2,1,0:T(8,128)S(1)}, u32[]{:S(2)}) copy-start(f32[3,32,512]{2,1,0:T(8,128)S(1)} %get-tuple-element.16) | copy-start | bytes 589828
  195.5 7.4 %collective-permute-start = (bf16[3,32,512]{2,1,0:T(8,128)(2,1)S(1)}, bf16[3,32,512]{2,1,0:T(8,128)(2,1)S(1)}, u32[]{:S(2)}, u32[]{:S(2)}) collective-permute-start(bf16[3,32,512]{2,1,0:T(8,128)(2,1)S(1)} %divide_convert_fusion), channel_id=1, source_target_pairs={{0,4},{4,8},{8,12},{12,16},{16,20},{20,24},{24,28},{28,0},{1,5},{5... | collective-permute-start | bytes 294920 | tf_op jit(solution)/shard_map/ppermute | solution.py:12
  202.9 7.3 %collective-permute-start.1 = (bf16[3,32,512]{2,1,0:T(8,128)(2,1)S(1)}, bf16[3,32,512]{2,1,0:T(8,128)(2,1)S(1)}, u32[]{:S(2)}, u32[]{:S(2)}) collective-permute-start(bf16[3,32,512]{2,1,0:T(8,128)(2,1)S(1)} %collective-permute-done), channel_id=1, source_target_pairs={{0,4},{4,8},{8,12},{12,16},{16,20},{20,24},{24,28},{28,0},{1,5},{5... | collective-permute-start | bytes 294920 | tf_op jit(solution)/shard_map/ppermute | solution.py:12
  210.2 7.3 %collective-permute-start.2 = (bf16[3,32,512]{2,1,0:T(8,128)(2,1)S(1)}, bf16[3,32,512]{2,1,0:T(8,128)(2,1)S(1)}, u32[]{:S(2)}, u32[]{:S(2)}) collective-permute-start(bf16[3,32,512]{2,1,0:T(8,128)(2,1)S(1)} %collective-permute-done.1), channel_id=1, source_target_pairs={{0,4},{4,8},{8,12},{12,16},{16,20},{20,24},{24,28},{28,0},{1,5},{5... | collective-permute-start | bytes 294920 | tf_op jit(solution)/shard_map/ppermute | solution.py:12
  217.5 7.4 %collective-permute-start.3 = (bf16[3,32,512]{2,1,0:T(8,128)(2,1)S(1)}, bf16[3,32,512]{2,1,0:T(8,128)(2,1)S(1)}, u32[]{:S(2)}, u32[]{:S(2)}) collective-permute-start(bf16[3,32,512]{2,1,0:T(8,128)(2,1)S(1)} %collective-permute-done.2), channel_id=1, source_target_pairs={{0,4},{4,8},{8,12},{12,16},{16,20},{20,24},{24,28},{28,0},{1,5},{5... | collective-permute-start | bytes 294920 | tf_op jit(solution)/shard_map/ppermute | solution.py:12
  224.9 8.2 %collective-permute-start.4 = (bf16[3,32,512]{2,1,0:T(8,128)(2,1)S(1)}, bf16[3,32,512]{2,1,0:T(8,128)(2,1)S(1)}, u32[]{:S(2)}, u32[]{:S(2)}) collective-permute-start(bf16[3,32,512]{2,1,0:T(8,128)(2,1)S(1)} %collective-permute-done.3), channel_id=1, source_target_pairs={{0,4},{4,8},{8,12},{12,16},{16,20},{20,24},{24,28},{28,0},{1,5},{5... | collective-permute-start | bytes 294920 | tf_op jit(solution)/shard_map/ppermute | solution.py:12
  225.3 22.4 %copy-start.4 = (f32[3,256,512]{2,1,0:T(8,128)S(1)}, f32[3,256,512]{2,1,0:T(8,128)}, u32[]{:S(2)}) copy-start(f32[3,256,512]{2,1,0:T(8,128)} %param.13) | copy-start | bytes 4718596
  233.1 7.3 %collective-permute-start.5 = (bf16[3,32,512]{2,1,0:T(8,128)(2,1)S(1)}, bf16[3,32,512]{2,1,0:T(8,128)(2,1)S(1)}, u32[]{:S(2)}, u32[]{:S(2)}) collective-permute-start(bf16[3,32,512]{2,1,0:T(8,128)(2,1)S(1)} %collective-permute-done.4), channel_id=1, source_target_pairs={{0,4},{4,8},{8,12},{12,16},{16,20},{20,24},{24,28},{28,0},{1,5},{5... | collective-permute-start | bytes 294920 | tf_op jit(solution)/shard_map/ppermute | solution.py:12
  240.4 7.3 %collective-permute-start.6 = (bf16[3,32,512]{2,1,0:T(8,128)(2,1)S(1)}, bf16[3,32,512]{2,1,0:T(8,128)(2,1)S(1)}, u32[]{:S(2)}, u32[]{:S(2)}) collective-permute-start(bf16[3,32,512]{2,1,0:T(8,128)(2,1)S(1)} %collective-permute-done.5), channel_id=1, source_target_pairs={{0,4},{4,8},{8,12},{12,16},{16,20},{20,24},{24,28},{28,0},{1,5},{5... | collective-permute-start | bytes 294920 | tf_op jit(solution)/shard_map/ppermute | solution.py:12
Sparse Core Ops, SparseCore 0:
  10.2 62.7 all-gather.2
  91.1 61.9 reduce-scatter.1
  250.6 97.0 all-gather.4
